TPU v7x, 32 devices: a whole 2x2x4 slice. The times are simulated.
32 devices in a mesh: grp: 2 (over x), ep: 4 (over y, core), tp: 4 (over z).
Axes of the slice: x: 2, y: 2, z: 4, core: 2. Of those that a mesh axis runs over, the one named last changes fastest.
Arguments:
- tokens: bfloat16 [3072, 4096], P(('grp', 'ep'), 'tp'), parts along dimension 0
- pre_gain: float32 [4096], replicated, may hold values from 0.1 to 1.9
- out_gain: float32 [4096], P('tp'), may hold values from 0.1 to 1.9
- chosen: int32 [8, 4, 48], P(('grp', 'ep')), parts along dimension 0, may hold values from 0 to 383, as said below
- route_weight: float32 [8, 4, 48], P(('grp', 'ep')), parts along dimension 0, may hold values from 0.3 to 3
- expert_gate: bfloat16 [4, 4096, 3072], P('ep', None, 'tp'), may hold values from -0.09375 to 0.09375
- expert_up: bfloat16 [4, 4096, 3072], P('ep', None, 'tp'), may hold values from -0.09375 to 0.09375
- expert_down: bfloat16 [4, 3072, 4096], P('ep', 'tp'), may hold values from -0.109375 to 0.109375
Outputs:
- output: bfloat16 [3072, 4096], P(('grp', 'ep'), 'tp'), parts along dimension 0
There are 2 independent parts, one for each index of `grp`. A program takes and returns all parts, laid end to end along the dimension named above; an argument that names none is the same for every part. Nothing has to cross between parts.
Inputs may be any that keep to these rules, and one draw needn't show every extreme that they name: chosen[b, e, k] is the position, within block b of 384 tokens, of the k-th token that expert e takes from that block; the 48 positions of one block and one expert are all different.
All inputs are finite; a program needn't handle non-finite values.
Results may differ from a plain program's by a relative error of at most 0.0075.
Values may be sent and summed in bfloat16 or wider, within the bound.
No kernel may reach another device: no remote copies, remote signals or barrier semaphores. Data moves between devices by JAX's collectives and lax.ppermute only.
A program may use at most 64 MiB of HBM per device.

v0:
```python
import jax
import jax.numpy as jnp
from jax import lax
from jax.sharding import PartitionSpec as P

NORM_EPS = 1e-06


def shards(tokens, pre_gain, out_gain, chosen, route_weight, expert_gate, expert_up, expert_down):
    model_width = pre_gain.shape[0]
    shard_width = tokens.shape[1]
    tok_count = tokens.shape[0]
    chosen_here = chosen[0]
    experts_all = chosen_here.shape[0]
    slot_count = chosen_here.shape[1]
    resident = tokens.astype(jnp.float32)
    square_sum = lax.psum(jnp.sum(resident * resident, axis=1), "tp")
    row_scale = lax.rsqrt(square_sum / model_width + NORM_EPS)[:, None]
    gain_slice = lax.dynamic_slice_in_dim(
        pre_gain, lax.axis_index("tp") * shard_width, shard_width, 0
    )
    normed = (resident * row_scale * gain_slice).astype(jnp.bfloat16)
    outgoing = jnp.take(normed, chosen_here, axis=0)
    incoming = lax.all_to_all(outgoing, "ep", split_axis=0, concat_axis=0, tiled=True)
    picked_rows = lax.all_gather(incoming.reshape(-1, shard_width), "tp", axis=1, tiled=True)
    gate_act = jnp.dot(picked_rows, expert_gate[0], preferred_element_type=jnp.float32)
    up_act = jnp.dot(picked_rows, expert_up[0], preferred_element_type=jnp.float32)
    hidden = (jax.nn.silu(gate_act) * up_act).astype(jnp.bfloat16)
    down_shard = expert_down[0]
    summed = lax.psum_scatter(
        lax.dot_general(
            down_shard, hidden, (((0,), (1,)), ((), ())), preferred_element_type=jnp.float32
        ).astype(jnp.bfloat16),
        "tp",
        scatter_dimension=0,
        tiled=True,
    )
    expert_out = summed.reshape(shard_width, experts_all, slot_count)
    returned = lax.all_to_all(expert_out, "ep", split_axis=1, concat_axis=1, tiled=True)
    weighted = returned.astype(jnp.float32) * route_weight[0][None]
    flat_weighted = weighted.reshape(shard_width, experts_all * slot_count)
    update_cols = (
        jnp.zeros((shard_width, tok_count), jnp.float32)
        .at[:, chosen_here.reshape(-1)]
        .add(flat_weighted)
    )
    mixed_rows = resident + update_cols.T
    out_sum = lax.psum(jnp.sum(mixed_rows * mixed_rows, axis=1), "tp")
    out_scale = lax.rsqrt(out_sum / model_width + NORM_EPS)[:, None]
    return (mixed_rows * out_scale * out_gain).astype(jnp.bfloat16)


def solution(mesh):
    return jax.shard_map(
        shards,
        mesh=mesh,
        in_specs=(
            P(("grp", "ep"), "tp"),
            P(),
            P("tp"),
            P(("grp", "ep"), None, None),
            P(("grp", "ep"), None, None),
            P("ep", None, "tp"),
            P("ep", None, "tp"),
            P("ep", "tp", None),
        ),
        out_specs=P(("grp", "ep"), "tp"),
        check_vma=False,
    )
```

profile of v0, /device:TPU:0, one launch (start us, length us, event | category | flops | bytes accessed | tf_op | source)
XLA Modules:
  0.0 150.9 jit_solution(1247583569600255627)
XLA Ops:
  6.5 0.0 all-gather.2.cloned.1.call-start
  6.5 0.7 compare_select_fusion.1
  7.2 0.7 compare_and_fusion
  7.9 1.4 fusion.12
  9.3 13.5 %psum.14 = f32[384]{0:T(512)S(1)} all-reduce(f32[384]{0:T(512)S(1)} %fusion.12), channel_id=1, replica_groups=mesh['grp'=2,'ep'=4,'tp'=4] {'tp'}, use_global_device_ids=true, to_apply=%region_1.0 | all-reduce | flops 384 | bytes 3072 | tf_op jit(solution)/shard_map/psum | solution.py:17
  22.8 0.1 reshape.80
  22.9 0.7 dynamic_slice.3
  23.6 1.4 fusion.14
  24.9 1.0 gather_fusion
  26.0 0.1 broadcast_select_fusion
  26.1 10.5 %all_to_all.10 = bf16[4,48,1024]{2,1,0:T(8,128)(2,1)} all-to-all(bf16[4,48,1024]{2,1,0:T(8,128)(2,1)S(1)} %broadcast_select_fusion), channel_id=1, replica_groups=mesh['grp'=2,'ep'=4,'tp'=4] {'ep'}, dimensions={0} | all-to-all | bytes 786432 | tf_op jit(solution)/shard_map/all_to_all | solution.py:24
  36.5 0.0 all-gather.2.cloned.1.call-update
  36.6 0.0 reduce-scatter.2.cloned.1.call-start
  36.6 34.4 %all-gather.2.cloned.1.call-done = bf16[192,4096]{1,0:T(8,128)(2,1)} async-done(((bf16[192,1024]{1,0:T(8,128)(2,1)}), bf16[192,4096]{1,0:T(8,128)(2,1)}) %all-gather.2.cloned.1.call-update) | async-done | bytes 1572880 | tf_op jit(solution)/shard_map/all_gather | solution.py:25
  71.0 4.8 %fusion.4 = f32[192,768]{1,0:T(8,128)S(1)} fusion(bf16[192,4096]{1,0:T(8,128)(2,1)} %all-gather.2.cloned.1.call-done, bf16[1,4096,768]{2,1,0:T(8,128)(2,1)} %param.13), kind=kOutput, calls=%fused_computation.6 | convolution fusion | flops 1207959552 | bytes 8454144 | tf_op jit(solution)/shard_map/dot_general | solution.py:26
  75.8 0.0 copy-done.4
  75.8 9.3 %fusion.9 = bf16[4096,192]{0,1:T(8,128)(2,1)} fusion(bf16[1,768,4096]{2,1,0:T(8,128)(2,1)} %param.15, bf16[192,4096]{1,0:T(8,128)(2,1)S(1)} %copy-done.4, bf16[1,4096,768]{2,1,0:T(8,128)(2,1)} %param.14, f32[192,768]{1,0:T(8,128)S(1)} %fusion.4), kind=kOutput, calls=%fused_computation.9 | convolution fusion | flops 2417590272 | bytes 16318464 | tf_op jit(solution)/shard_map/dot_general | solution.py:31
  85.0 0.0 reduce-scatter.2.cloned.1.call-update
  85.1 34.4 %reduce-scatter.2.cloned.1.call-done = bf16[1024,192]{0,1:T(8,128)(2,1)} async-done(((bf16[4096,192]{0,1:T(8,128)(2,1)}), bf16[1024,192]{0,1:T(8,128)(2,1)}) %reduce-scatter.2.cloned.1.call-update) | async-done | bytes 393232 | tf_op jit(solution)/shard_map/reduce_scatter | solution.py:30
  119.5 3.5 %all-to-all-start.1 = ((bf16[1024,4,48]{0,2,1:T(8,128)(2,1)}), bf16[1024,4,48]{0,2,1:T(8,128)(2,1)S(1)}, u32[]{:S(2)}, u32[]{:S(2)}) async-start(bf16[1024,4,48]{0,2,1:T(8,128)(2,1)} %bitcast.48), calls=%async_computation.2 | async-start | bytes 786432 | tf_op jit(solution)/shard_map/all_to_all | solution.py:39
  123.0 0.0 copy-done.1
  123.0 0.0 copy-start
  123.0 0.1 reshape_squeeze.3
  123.1 7.3 %all-to-all-done.1 = bf16[1024,4,48]{0,2,1:T(8,128)(2,1)S(1)} async-done(((bf16[1024,4,48]{0,2,1:T(8,128)(2,1)}), bf16[1024,4,48]{0,2,1:T(8,128)(2,1)S(1)}, u32[]{:S(2)}, u32[]{:S(2)}) %all-to-all-start.1) | async-done | bytes 393248 | tf_op jit(solution)/shard_map/all_to_all | solution.py:39
  130.3 0.0 copy-done.3
  130.3 0.1 convert_multiply_fusion.2
  130.5 2.5 %scatter_custom_fusion = f32[1024,384]{0,1:T(8,128)S(1)} fusion(s32[192]{0:T(256)S(1)} %bitcast.50, f32[192,1024]{1,0:T(8,128)S(1)} %bitcast.47, f32[]{:T(128)} %constant.11.clone.1), kind=kCustom, calls=%fused_computation.21 | custom fusion | flops 196608 | bytes 1572868 | tf_op jit(solution)/shard_map/scatter-add | solution.py:45
  133.0 0.0 copy-start.2
  133.0 0.3 multiply_reduce_fusion
  133.3 9.6 %psum.15 = f32[384]{0:T(512)S(1)} all-reduce(f32[384]{0:T(512)S(1)} %multiply_reduce_fusion), channel_id=1, replica_groups=mesh['grp'=2,'ep'=4,'tp'=4] {'tp'}, use_global_device_ids=true, to_apply=%region_5.6 | all-reduce | flops 384 | bytes 3072 | tf_op jit(solution)/shard_map/psum | solution.py:48
  142.9 0.0 copy-done.2
  142.9 1.1 multiply_convert_fusion
  (8 shorter events, 0.0 us)
Async XLA Ops:
  6.5 64.5 %all-gather.2.cloned.1.call-start = ((), (), s32[]{:S(2)}) async-start(), calls=%async_computation.3 | async-start | bytes 1966080 | tf_op jit(solution)/shard_map/all_gather | solution.py:25
  36.6 82.9 %reduce-scatter.2.cloned.1.call-start = ((), (), s32[]{:S(2)}) async-start(), calls=%async_computation.4 | async-start | bytes 1966080 | tf_op jit(solution)/shard_map/reduce_scatter | solution.py:30
  71.0 4.8 %copy-start.4 = (bf16[192,4096]{1,0:T(8,128)(2,1)S(1)}, bf16[192,4096]{1,0:T(8,128)(2,1)}, u32[]{:S(2)}) copy-start(bf16[192,4096]{1,0:T(8,128)(2,1)} %all-gather.2.cloned.1.call-done) | copy-start | bytes 4718596
  85.0 37.9 %copy-start.1 = (s32[1,4,48]{2,1,0:T(4,128)S(1)}, s32[1,4,48]{2,1,0:T(4,128)}, u32[]{:S(2)}) copy-start(s32[1,4,48]{2,1,0:T(4,128)} %param.11) | copy-start | bytes 2308
  85.0 45.3 %copy-start.3 = (f32[1,4,48]{2,1,0:T(4,128)S(1)}, f32[1,4,48]{2,1,0:T(4,128)}, u32[]{:S(2)}) copy-start(f32[1,4,48]{2,1,0:T(4,128)} %param.12) | copy-start | bytes 2308
  119.5 10.8 %all-to-all-start.1 = ((bf16[1024,4,48]{0,2,1:T(8,128)(2,1)}), bf16[1024,4,48]{0,2,1:T(8,128)(2,1)S(1)}, u32[]{:S(2)}, u32[]{:S(2)}) async-start(bf16[1024,4,48]{0,2,1:T(8,128)(2,1)} %bitcast.48), calls=%async_computation.2 | async-start | bytes 786432 | tf_op jit(solution)/shard_map/all_to_all | solution.py:39
  123.0 10.0 %copy-start = (bf16[384,1024]{1,0:T(8,128)(2,1)S(1)}, bf16[384,1024]{1,0:T(8,128)(2,1)}, u32[]{:S(2)}) copy-start(bf16[384,1024]{1,0:T(8,128)(2,1)} %param.8) | copy-start | bytes 2359300
  133.0 9.9 %copy-start.2 = (f32[1024]{0:T(1024)S(1)}, f32[1024]{0:T(1024)}, u32[]{:S(2)}) copy-start(f32[1024]{0:T(1024)} %param.10) | copy-start | bytes 12292
Sparse Core Ops, SparseCore 0:
  36.7 34.2 all-gather.1
  85.2 34.2 reduce-scatter.1
where the time goes:
time: 151 us
  waiting for transfers between devices  76.1 us (50%)
  blocking collectives  33.6 us (22%)
  matrix products  14 us (9%)
  between operations  13.5 us (9%)
  other arithmetic  8.29 us (5%)
  starting transfers between devices  3.5 us (2%)
  local copies, waits for them, and re-layouts  1.9 us (1%)
    reduce_scatter x1, waiting for transfers between devices, shards(): lax.psum_scatter(lax.dot_general(down_shard, hidden, (((0,), (1,)), ((),...  34.4 us
    all_gather x1, waiting for transfers between devices, shards(): lax.all_gather(incoming.reshape(-1, shard_width), 'tp', axis=1, tiled=True)  34.4 us
    psum x1, blocking collectives, shards(): square_sum = lax.psum(jnp.sum(resident * resident, axis=1), 'tp')  13.5 us
    all_to_all x1, blocking collectives, shards(): lax.all_to_all(outgoing, 'ep', split_axis=0, concat_axis=0, tiled=True)  10.5 us
    psum x1, blocking collectives, shards(): out_sum = lax.psum(jnp.sum(mixed_rows * mixed_rows, axis=1), 'tp')  9.64 us
    dot_general x1, matrix products, shards(): lax.dot_general(down_shard, hidden, (((0,), (1,)), ((), ())), preferred_e...  9.25 us
    all_to_all x1, waiting for transfers between devices, shards(): lax.all_to_all(expert_out, 'ep', split_axis=1, concat_axis=1, tiled=True)  7.26 us
    dot_general x1, matrix products, shards(): jnp.dot(picked_rows, expert_gate[0], preferred_element_type=jnp.float32)  4.76 us
  transfers between devices with their start and end apart: 3, of which 3 were waited for; matrix products, arithmetic and copies ran while one was open for 0% of the time, Pallas kernels for 0%

commit v1 on v0

--- a/solution.py
+++ b/solution.py
@@ -4,6 +4,29 @@
 from jax.sharding import PartitionSpec as P
 
 NORM_EPS = 1e-06
+
+
+def cut_along(shard, dim, length):
+    dims = shard.shape
+    blocks = shard.reshape(*dims[:dim], length, dims[dim] // length, *dims[dim + 1 :])
+    return jnp.moveaxis(blocks, dim, 0)
+
+
+def joined_along(pieces, dim):
+    dims = list(pieces.shape[1:])
+    dims[dim] *= pieces.shape[0]
+    return jnp.moveaxis(pieces, 0, dim).reshape(dims)
+
+
+def exchange_in_pairs(shard, axis, split_dim, concat_dim):
+    length, index = (lax.axis_size(axis), lax.axis_index(axis))
+    parts = cut_along(shard, split_dim, length)
+    gathered = [parts[index]]
+    for step in range(1, length):
+        sent = parts[index ^ step]
+        gathered.append(lax.ppermute(sent, axis, [(i, i ^ step) for i in range(length)]))
+    parts = jnp.stack(gathered)[index ^ jnp.arange(length)]
+    return joined_along(parts, concat_dim)
 
 
 def shards(tokens, pre_gain, out_gain, chosen, route_weight, expert_gate, expert_up, expert_down):
@@ -36,7 +59,7 @@
         tiled=True,
     )
     expert_out = summed.reshape(shard_width, experts_all, slot_count)
-    returned = lax.all_to_all(expert_out, "ep", split_axis=1, concat_axis=1, tiled=True)
+    returned = exchange_in_pairs(expert_out, "ep", 1, 1)
     weighted = returned.astype(jnp.float32) * route_weight[0][None]
     flat_weighted = weighted.reshape(shard_width, experts_all * slot_count)
     update_cols = (

time: 151 us -> 150 us (level)
  waiting for transfers between devices: 76.1 us -> 73.4 us
  local copies, waits for them, and re-layouts: 1.9 us -> 4.26 us
  starting transfers between devices: 3.5 us -> 1.97 us
    all_to_all x1 -> x0, waiting for transfers between devices: 7.26 us -> none  [shards(): lax.all_to_all(expert_out, 'ep', split_axis=1, concat_axis=1, tiled=True)]
    ppermute x0 -> x3, waiting for transfers between devices: none -> 5.34 us  [exchange_in_pairs(): lax.ppermute(sent, axis, [(i, i ^ step) for i in range(length)])]
    all_to_all x1 -> x0, starting transfers between devices: 3.46 us -> none  [shards(): lax.all_to_all(expert_out, 'ep', split_axis=1, concat_axis=1, tiled=True)]
    ppermute x0 -> x3, starting transfers between devices: none -> 1.93 us  [exchange_in_pairs(): lax.ppermute(sent, axis, [(i, i ^ step) for i in range(length)])]
  transfers between devices with their start and end apart: 3 -> 5, of which waited for: 3 -> 4; matrix products, arithmetic and copies ran while one was open for 0% -> 0% of each run, Pallas kernels for 0% -> 0%
where the time goes in v1:
time: 150 us; the launch traced here: 149 us
  waiting for transfers between devices  73.4 us (49%)
  blocking collectives  33.6 us (22%)
  matrix products  14 us (9%)
  between operations  13.5 us (9%)
  other arithmetic  8.48 us (6%)
  local copies, waits for them, and re-layouts  4.26 us (3%)
  starting transfers between devices  1.97 us (1%)
    all_gather x1, waiting for transfers between devices, shards(): lax.all_gather(incoming.reshape(-1, shard_width), 'tp', axis=1, tiled=True)  34.4 us
    reduce_scatter x1, waiting for transfers between devices, shards(): lax.psum_scatter(lax.dot_general(down_shard, hidden, (((0,), (1,)), ((),...  33.6 us
    psum x1, blocking collectives, shards(): square_sum = lax.psum(jnp.sum(resident * resident, axis=1), 'tp')  13.5 us
    all_to_all x1, blocking collectives, shards(): lax.all_to_all(outgoing, 'ep', split_axis=0, concat_axis=0, tiled=True)  10.5 us
    psum x1, blocking collectives, shards(): out_sum = lax.psum(jnp.sum(mixed_rows * mixed_rows, axis=1), 'tp')  9.64 us
    dot_general x1, matrix products, shards(): lax.dot_general(down_shard, hidden, (((0,), (1,)), ((), ())), preferred_e...  9.25 us
    ppermute x3, waiting for transfers between devices, exchange_in_pairs(): lax.ppermute(sent, axis, [(i, i ^ step) for i in range(length)])  5.34 us
    dot_general x1, matrix products, shards(): jnp.dot(picked_rows, expert_gate[0], preferred_element_type=jnp.float32)  4.76 us
  transfers between devices with their start and end apart: 5, of which 4 were waited for; matrix products, arithmetic and copies ran while one was open for 0% of the time, Pallas kernels for 0%

profile of v1, /device:TPU:0, one launch (start us, length us, event | category | flops | bytes accessed | tf_op | source)
XLA Modules:
  0.0 149.2 jit_solution(679117225496469679)
XLA Ops:
  6.5 0.7 compare_select_fusion.1
  7.2 0.7 compare_and_fusion
  7.9 1.4 fusion.12
  9.3 13.5 %psum.14 = f32[384]{0:T(512)S(1)} all-reduce(f32[384]{0:T(512)S(1)} %fusion.12), channel_id=1, replica_groups=mesh['grp'=2,'ep'=4,'tp'=4] {'tp'}, use_global_device_ids=true, to_apply=%region_1.0 | all-reduce | flops 384 | bytes 3072 | tf_op jit(solution)/shard_map/psum | solution.py:40
  22.8 0.1 reshape.103
  22.9 0.7 dynamic_slice.4
  23.6 1.4 fusion.14
  24.9 1.0 gather_fusion
  26.0 0.1 broadcast_select_fusion
  26.1 10.5 %all_to_all.5 = bf16[4,48,1024]{2,1,0:T(8,128)(2,1)} all-to-all(bf16[4,48,1024]{2,1,0:T(8,128)(2,1)S(1)} %broadcast_select_fusion), channel_id=1, replica_groups=mesh['grp'=2,'ep'=4,'tp'=4] {'ep'}, dimensions={0} | all-to-all | bytes 786432 | tf_op jit(solution)/shard_map/all_to_all | solution.py:47
  36.6 0.0 reduce-scatter.2.cloned.1.call-start
  36.6 34.4 %all-gather.2.cloned.1.call-done = bf16[192,4096]{1,0:T(8,128)(2,1)} async-done(((bf16[192,1024]{1,0:T(8,128)(2,1)}), bf16[192,4096]{1,0:T(8,128)(2,1)}) %all-gather.2.cloned.1.call-update) | async-done | bytes 1572880 | tf_op jit(solution)/shard_map/all_gather | solution.py:48
  71.0 4.8 %fusion.4 = f32[192,768]{1,0:T(8,128)S(1)} fusion(bf16[192,4096]{1,0:T(8,128)(2,1)} %all-gather.2.cloned.1.call-done, bf16[1,4096,768]{2,1,0:T(8,128)(2,1)} %param.13), kind=kOutput, calls=%fused_computation.7 | convolution fusion | flops 1207959552 | bytes 8454144 | tf_op jit(solution)/shard_map/dot_general | solution.py:49
  75.8 9.3 %fusion.9 = bf16[4096,192]{0,1:T(8,128)(2,1)} fusion(bf16[1,768,4096]{2,1,0:T(8,128)(2,1)} %param.15, bf16[192,4096]{1,0:T(8,128)(2,1)S(1)} %copy-done.4, bf16[1,4096,768]{2,1,0:T(8,128)(2,1)} %param.14, f32[192,768]{1,0:T(8,128)S(1)} %fusion.4), kind=kOutput, calls=%fused_computation.10 | convolution fusion | flops 2417590272 | bytes 16318464 | tf_op jit(solution)/shard_map/dot_general | solution.py:54
  85.1 0.7 copy-done.1
  85.7 0.1 reshape_squeeze.3
  85.8 0.1 mul.67
  85.9 33.6 %reduce-scatter.2.cloned.1.call-done = bf16[1024,192]{0,1:T(8,128)(2,1)} async-done(((bf16[4096,192]{0,1:T(8,128)(2,1)}), bf16[1024,192]{0,1:T(8,128)(2,1)}) %reduce-scatter.2.cloned.1.call-update) | async-done | bytes 393232 | tf_op jit(solution)/shard_map/reduce_scatter | solution.py:53
  119.5 1.1 dynamic-slice_bitcast_fusion.3
  120.6 0.6 collective-permute-start.2
  121.2 1.0 collective-permute-start.1
  122.2 0.3 collective-permute-start
  122.5 3.2 %collective-permute-done.2 = bf16[1024,1,48]{0,2,1:T(8,128)(2,1)S(1)} collective-permute-done((bf16[1024,1,48]{0,2,1:T(8,128)(2,1)S(1)}, bf16[1024,1,48]{0,2,1:T(8,128)(2,1)S(1)}, u32[]{:S(2)}, u32[]{:S(2)}) %collective-permute-start.2) | collective-permute-done | bytes 98336 | tf_op jit(solution)/shard_map/ppermute | solution.py:27
  125.7 2.1 %collective-permute-done.1 = bf16[1024,1,48]{0,2,1:T(8,128)(2,1)S(1)} collective-permute-done((bf16[1024,1,48]{0,2,1:T(8,128)(2,1)S(1)}, bf16[1024,1,48]{0,2,1:T(8,128)(2,1)S(1)}, u32[]{:S(2)}, u32[]{:S(2)}) %collective-permute-start.1) | collective-permute-done | bytes 98336 | tf_op jit(solution)/shard_map/ppermute | solution.py:27
  127.8 0.1 maximum_bitcast_fusion
  127.9 0.6 gather_fusion.1
  128.5 0.1 bitcast_convert_fusion
  128.6 0.1 bitcast_multiply_fusion
  128.7 2.5 %scatter_custom_fusion = f32[1024,384]{0,1:T(8,128)S(1)} fusion(s32[192]{0:T(256)S(1)} %bitcast.72, f32[1024,192]{0,1:T(8,128)S(1)} %bitcast_multiply_fusion, f32[]{:T(128)} %constant.16.clone.1), kind=kCustom, calls=%fused_computation.22 | custom fusion | flops 196608 | bytes 2359300 | tf_op jit(solution)/shard_map/scatter-add | solution.py:68
  131.3 0.3 multiply_reduce_fusion
  131.6 9.6 %psum.15 = f32[384]{0:T(512)S(1)} all-reduce(f32[384]{0:T(512)S(1)} %multiply_reduce_fusion), channel_id=1, replica_groups=mesh['grp'=2,'ep'=4,'tp'=4] {'tp'}, use_global_device_ids=true, to_apply=%region_5.6 | all-reduce | flops 384 | bytes 3072 | tf_op jit(solution)/shard_map/psum | solution.py:71
  141.2 1.1 multiply_convert_fusion
  (19 shorter events, 0.1 us)
Async XLA Ops:
  6.5 64.5 %all-gather.2.cloned.1.call-start = ((), (), s32[]{:S(2)}) async-start(), calls=%async_computation.2 | async-start | bytes 1966080 | tf_op jit(solution)/shard_map/all_gather | solution.py:48
  36.6 82.9 %reduce-scatter.2.cloned.1.call-start = ((), (), s32[]{:S(2)}) async-start(), calls=%async_computation.3 | async-start | bytes 1966080 | tf_op jit(solution)/shard_map/reduce_scatter | solution.py:53
  71.0 4.8 %copy-start.4 = (bf16[192,4096]{1,0:T(8,128)(2,1)S(1)}, bf16[192,4096]{1,0:T(8,128)(2,1)}, u32[]{:S(2)}) copy-start(bf16[192,4096]{1,0:T(8,128)(2,1)} %all-gather.2.cloned.1.call-done) | copy-start | bytes 4718596
  85.0 0.7 copy-start.1
  85.0 0.8 copy-start.3
  120.6 5.1 %collective-permute-start.2 = (bf16[1024,1,48]{0,2,1:T(8,128)(2,1)S(1)}, bf16[1024,1,48]{0,2,1:T(8,128)(2,1)S(1)}, u32[]{:S(2)}, u32[]{:S(2)}) collective-permute-start(bf16[1024,1,48]{0,2,1:T(8,128)(2,1)S(1)} %get-tuple-element.6), channel_id=1, source_target_pairs={{0,12},{4,8},{8,4},{12,0},{1,13},{5,9},{9,5},{13,1},{2,14},{6,10},... | collective-permute-start | bytes 294920 | tf_op jit(solution)/shard_map/ppermute | solution.py:27
  121.2 6.7 %collective-permute-start.1 = (bf16[1024,1,48]{0,2,1:T(8,128)(2,1)S(1)}, bf16[1024,1,48]{0,2,1:T(8,128)(2,1)S(1)}, u32[]{:S(2)}, u32[]{:S(2)}) collective-permute-start(bf16[1024,1,48]{0,2,1:T(8,128)(2,1)S(1)} %get-tuple-element.7), channel_id=1, source_target_pairs={{0,8},{4,12},{8,0},{12,4},{1,9},{5,13},{9,1},{13,5},{2,10},{6,14},... | collective-permute-start | bytes 294920 | tf_op jit(solution)/shard_map/ppermute | solution.py:27
  122.2 5.7 %collective-permute-start = (bf16[1024,1,48]{0,2,1:T(8,128)(2,1)S(1)}, bf16[1024,1,48]{0,2,1:T(8,128)(2,1)S(1)}, u32[]{:S(2)}, u32[]{:S(2)}) collective-permute-start(bf16[1024,1,48]{0,2,1:T(8,128)(2,1)S(1)} %get-tuple-element.8), channel_id=1, source_target_pairs={{0,4},{4,0},{8,12},{12,8},{1,5},{5,1},{9,13},{13,9},{2,6},{6,2},{1... | collective-permute-start | bytes 294920 | tf_op jit(solution)/shard_map/ppermute | solution.py:27
  128.7 2.6 %copy-start = (bf16[384,1024]{1,0:T(8,128)(2,1)S(1)}, bf16[384,1024]{1,0:T(8,128)(2,1)}, u32[]{:S(2)}) copy-start(bf16[384,1024]{1,0:T(8,128)(2,1)} %param.8) | copy-start | bytes 2359300
  131.3 9.9 %copy-start.2 = (f32[1024]{0:T(1024)S(1)}, f32[1024]{0:T(1024)}, u32[]{:S(2)}) copy-start(f32[1024]{0:T(1024)} %param.10) | copy-start | bytes 12292
Sparse Core Ops, SparseCore 0:
  36.7 34.2 all-gather.1
  85.2 34.2 reduce-scatter.1
